TPU v7x, 32 devices: a whole 2x2x4 slice. The times are simulated.
32 devices in a mesh: rep: 2 (over x), fs: 4 (over z), tp: 4 (over y, core).
Axes of the slice: x: 2, y: 2, z: 4, core: 2. Of those that a mesh axis runs over, the one named last changes fastest.
Arguments:
- tokens: bfloat16 [4096, 2048], P(('rep', 'fs', 'tp')), may hold values from -6 to 6
- norm1_gain: float32 [2048], replicated, may hold values from 0.1 to 1.9
- in_weight: bfloat16 [2048, 1024], P('fs', 'tp'), may hold values from -0.125 to 0.125
- group_weight: bfloat16 [8, 128, 128], P('tp'), may hold values from -0.5 to 0.5
- pool_scale: float32 [1024], P('tp'), may hold values from 0.1 to 1.9
- out_weight: bfloat16 [1024, 2048], P('tp', 'fs'), may hold values from -0.1875 to 0.1875
- norm2_gain: float32 [2048], replicated, may hold values from 0.1 to 1.9
- up_weight: bfloat16 [2048, 8192], P('fs', 'tp'), may hold values from -0.125 to 0.125
- down_weight: bfloat16 [8192, 2048], P('tp', 'fs'), may hold values from -0.0625 to 0.0625
Outputs:
- layer_out: bfloat16 [4096, 2048], P(('rep', 'fs', 'tp'))
All inputs are finite; a program needn't handle non-finite values.
Results may differ from a plain program's by a relative error of at most 0.02.
Values may be sent and summed in bfloat16 or wider, within the bound.
A program may use at most 128 MiB of HBM per device.

v0:
```python
import jax
import jax.numpy as jnp
from jax import lax
from jax.sharding import PartitionSpec as P

GROUP_DIM = 128


epsilon = 1e-06


def rms_norm(values, gain):
    scale = lax.rsqrt(jnp.mean(values * values, axis=-1, keepdims=True) + epsilon)
    return values * scale * gain


def shifted(values, offset):
    return jnp.pad(values, ((offset, 0), (0, 0)))[: values.shape[0]]


def mix_groups(projected, group_weight, pool_scale):
    length = projected.shape[0]
    local_groups = group_weight.shape[0]
    values = projected.astype(jnp.float32)
    level_sums = []
    running = values
    offset = 1
    for level in range(4):
        running = running + shifted(running, offset)
        offset = offset * 2
        level_sums.append(running)
    first_group = lax.axis_index("tp") * local_groups
    group_level = (first_group + jnp.arange(local_groups, dtype=jnp.int32)) % 4
    column_level = jnp.repeat(group_level, GROUP_DIM)[None, :]
    position = jnp.arange(length, dtype=jnp.int32)[:, None]
    window_mean = jnp.zeros_like(values)
    for level in range(4):
        count = jnp.minimum(position + 1, 2 ** (level + 1)).astype(jnp.float32)
        window_mean = jnp.where(column_level == level, level_sums[level] / count, window_mean)
    pooled = (window_mean - values).astype(jnp.bfloat16).reshape(length, local_groups, GROUP_DIM)
    mapped = jnp.einsum("sgc,gcd->sgd", pooled, group_weight, preferred_element_type=jnp.float32)
    return (mapped.reshape(length, local_groups * GROUP_DIM) * pool_scale).astype(jnp.bfloat16)


def local(
    tokens,
    norm1_gain,
    in_weight,
    group_weight,
    pool_scale,
    out_weight,
    norm2_gain,
    up_weight,
    down_weight,
):
    stream = tokens.astype(jnp.float32)
    normed = rms_norm(stream, norm1_gain).astype(jnp.bfloat16)
    in_local = lax.all_gather(in_weight, "fs", axis=0, tiled=True)
    projected = jnp.dot(
        lax.all_gather(normed, "tp", axis=0, tiled=True),
        in_local,
        preferred_element_type=jnp.float32,
    ).astype(jnp.bfloat16)
    pool_out = mix_groups(projected, group_weight, pool_scale)
    out_local = lax.all_gather(out_weight, "fs", axis=1, tiled=True)
    block_rows = pool_out
    mixed = lax.psum_scatter(
        jnp.dot(block_rows, out_local, preferred_element_type=jnp.float32).astype(jnp.bfloat16),
        "tp",
        scatter_dimension=0,
        tiled=True,
    ).astype(jnp.float32)
    mixed_stream = stream + mixed
    normed_two = rms_norm(mixed_stream, norm2_gain).astype(jnp.bfloat16)
    up_local = lax.all_gather(up_weight, "fs", axis=0, tiled=True)
    upper = jnp.dot(
        lax.all_gather(normed_two, "tp", axis=0, tiled=True),
        up_local,
        preferred_element_type=jnp.float32,
    )
    hidden = jnp.square(jax.nn.relu(upper)).astype(jnp.bfloat16)
    down_local = lax.all_gather(down_weight, "fs", axis=1, tiled=True)
    block_rows = hidden
    channel_sum = lax.psum_scatter(
        jnp.dot(block_rows, down_local, preferred_element_type=jnp.float32).astype(jnp.bfloat16),
        "tp",
        scatter_dimension=0,
        tiled=True,
    ).astype(jnp.float32)
    return (mixed_stream + channel_sum).astype(jnp.bfloat16)


def solution(mesh):
    in_specs = (
        P(("rep", "fs", "tp"), None),
        P(),
        P("fs", "tp"),
        P("tp", None, None),
        P("tp"),
        P("tp", "fs"),
        P(),
        P("fs", "tp"),
        P("tp", "fs"),
    )
    out_specs = P(("rep", "fs", "tp"), None)
    return jax.shard_map(local, mesh=mesh, in_specs=in_specs, out_specs=out_specs, check_vma=False)
```

profile of v0, /device:TPU:29, one launch (start us, length us, event | category | flops | bytes accessed | tf_op | source)
XLA Modules:
  0.0 505.5 jit_solution(7314951836628832567)
XLA Ops:
  6.5 0.0 copy-start
  6.5 0.0 all-gather.9.cloned.1.call-start
  6.5 0.7 all-gather.9.cloned.1.call-update
  7.3 0.0 all-gather.7.cloned.1.call-start
  7.3 1.2 fusion.1
  8.5 2.0 fusion.3
  10.6 0.0 all-gather.7.cloned.1.call-update
  10.6 0.0 all-gather.11.cloned.1.call-start
  10.6 0.7 all-gather.11.cloned.1.call-update
  11.3 0.0 reduce-scatter.3.cloned.1.call-start
  11.5 0.1 broadcast_bitcast_fusion
  11.5 0.1 broadcast_bitcast_fusion.1
  11.6 0.1 broadcast_bitcast_fusion.2
  11.7 0.1 broadcast_bitcast_fusion.3
  11.7 24.7 %all-gather.9.cloned.1.call-done = bf16[2048,256]{1,0:T(8,128)(2,1)} async-done(((bf16[512,256]{1,0:T(8,128)(2,1)}), bf16[2048,256]{1,0:T(8,128)(2,1)}) %all-gather.9.cloned.1.call-update) | async-done | bytes 1048592 | tf_op jit(solution)/shard_map/all_gather | solution.py:58
  36.4 24.5 %all-gather.7.cloned.1.call-done = bf16[512,2048]{1,0:T(8,128)(2,1)} async-done(((bf16[128,2048]{1,0:T(8,128)(2,1)}), bf16[512,2048]{1,0:T(8,128)(2,1)}) %all-gather.7.cloned.1.call-update) | async-done | bytes 2097168 | tf_op jit(solution)/shard_map/all_gather | solution.py:60
  60.9 2.6 fusion
  63.4 0.1 fusion.4
  63.5 0.1 fusion.5
  63.5 0.1 fusion.6
  63.6 0.0 copy-done
  63.6 0.0 copy-start.4
  63.6 0.7 fusion.13
  64.3 0.0 copy-done.4
  64.3 0.1 fusion.11
  64.4 25.1 %all-gather.11.cloned.1.call-done = bf16[256,2048]{1,0:T(8,128)(2,1)} async-done(((bf16[256,512]{1,0:T(8,128)(2,1)}), bf16[256,2048]{1,0:T(8,128)(2,1)}) %all-gather.11.cloned.1.call-update) | async-done | bytes 1048592 | tf_op jit(solution)/shard_map/all_gather | solution.py:65
  89.5 3.3 convolution_convert_fusion
  92.8 0.0 reduce-scatter.3.cloned.1.call-update
  92.8 0.0 all-gather.13.cloned.1.call-start
  92.9 31.0 %reduce-scatter.3.cloned.1.call-done = bf16[128,2048]{1,0:T(8,128)(2,1)} async-done(((bf16[512,2048]{1,0:T(8,128)(2,1)}), bf16[128,2048]{1,0:T(8,128)(2,1)}) %reduce-scatter.3.cloned.1.call-update) | async-done | bytes 524304 | tf_op jit(solution)/shard_map/reduce_scatter | solution.py:67
  123.9 0.0 copy-done.1
  123.9 1.3 multiply_reduce_fusion
  125.2 0.0 copy-done.3
  125.2 2.0 multiply_convert_fusion.1
  127.3 0.0 all-gather.13.cloned.1.call-update
  127.3 0.0 all-gather.15.cloned.1.call-start
  127.4 0.5 all-gather.15.cloned.1.call-update
  127.9 0.0 all-gather.17.cloned.1.call-start
  127.9 0.7 all-gather.17.cloned.1.call-update
  128.6 0.0 reduce-scatter.5.cloned.1.call-start
  128.7 21.9 %all-gather.13.cloned.1.call-done = bf16[512,2048]{1,0:T(8,128)(2,1)} async-done(((bf16[128,2048]{1,0:T(8,128)(2,1)}), bf16[512,2048]{1,0:T(8,128)(2,1)}) %all-gather.13.cloned.1.call-update) | async-done | bytes 2097168 | tf_op jit(solution)/shard_map/all_gather | solution.py:77
  150.6 148.9 %all-gather.15.cloned.1.call-done = bf16[2048,2048]{1,0:T(8,128)(2,1)} async-done(((bf16[512,2048]{1,0:T(8,128)(2,1)}), bf16[2048,2048]{1,0:T(8,128)(2,1)}) %all-gather.15.cloned.1.call-update) | async-done | bytes 8388624 | tf_op jit(solution)/shard_map/all_gather | solution.py:75
  299.5 149.4 %all-gather.17.cloned.1.call-done = bf16[2048,2048]{1,0:T(8,128)(2,1)} async-done(((bf16[2048,512]{1,0:T(8,128)(2,1)}), bf16[2048,2048]{1,0:T(8,128)(2,1)}) %all-gather.17.cloned.1.call-update) | async-done | bytes 8388624 | tf_op jit(solution)/shard_map/all_gather | solution.py:82
  448.9 16.5 %convolution_convert_fusion.1 = bf16[512,2048]{1,0:T(8,128)(2,1)} fusion(bf16[2048,2048]{1,0:T(8,128)(2,1)} %all-gather.17.cloned.1.call-done, bf16[512,2048]{1,0:T(8,128)(2,1)} %all-gather.13.cloned.1.call-done, bf16[2048,2048]{1,0:T(8,128)(2,1)} %all-gather.15.cloned.1.call-done), kind=kOutput, calls=%fused_computation.2 | convolution fusion | flops 8594128896 | bytes 20971520 | tf_op jit(solution)/shard_map/dot_general | solution.py:85
  465.4 0.0 reduce-scatter.5.cloned.1.call-update
  465.4 31.1 %reduce-scatter.5.cloned.1.call-done = bf16[128,2048]{1,0:T(8,128)(2,1)} async-done(((bf16[512,2048]{1,0:T(8,128)(2,1)}), bf16[128,2048]{1,0:T(8,128)(2,1)}) %reduce-scatter.5.cloned.1.call-update) | async-done | bytes 524304 | tf_op jit(solution)/shard_map/reduce_scatter | solution.py:84
  496.6 0.0 copy-done.2
  496.6 2.1 add_convert_fusion
  (9 shorter events, 0.1 us)
Async XLA Ops:
  6.5 57.1 %copy-start = (bf16[2,128,128]{2,1,0:T(8,128)(2,1)S(1)}, bf16[2,128,128]{2,1,0:T(8,128)(2,1)}, u32[]{:S(2)}) copy-start(bf16[2,128,128]{2,1,0:T(8,128)(2,1)} %param.12) | copy-start | bytes 196612
  6.5 29.9 %all-gather.9.cloned.1.call-start = ((), (), s32[]{:S(2)}) async-start(), calls=%async_computation.3 | async-start | bytes 1310720 | tf_op jit(solution)/shard_map/all_gather | solution.py:58
  7.3 53.6 %all-gather.7.cloned.1.call-start = ((), (), s32[]{:S(2)}) async-start(), calls=%async_computation.2 | async-start | bytes 2621440 | tf_op jit(solution)/shard_map/all_gather | solution.py:60
  10.6 78.9 %all-gather.11.cloned.1.call-start = ((), (), s32[]{:S(2)}) async-start(), calls=%async_computation.4 | async-start | bytes 1310720 | tf_op jit(solution)/shard_map/all_gather | solution.py:65
  11.3 112.6 %reduce-scatter.3.cloned.1.call-start = ((), (), s32[]{:S(2)}) async-start(), calls=%async_computation.5 | async-start | bytes 2621440 | tf_op jit(solution)/shard_map/reduce_scatter | solution.py:67
  63.6 0.7 copy-start.4
  92.8 31.1 %copy-start.1 = (bf16[128,2048]{1,0:T(8,128)(2,1)S(1)}, bf16[128,2048]{1,0:T(8,128)(2,1)}, u32[]{:S(2)}) copy-start(bf16[128,2048]{1,0:T(8,128)(2,1)} %param.9) | copy-start | bytes 1572868
  92.8 32.4 %copy-start.3 = (f32[2048]{0:T(1024)S(1)}, f32[2048]{0:T(1024)}, u32[]{:S(2)}) copy-start(f32[2048]{0:T(1024)} %param.15) | copy-start | bytes 24580
  92.8 57.7 %all-gather.13.cloned.1.call-start = ((), (), s32[]{:S(2)}) async-start(), calls=%async_computation.6 | async-start | bytes 2621440 | tf_op jit(solution)/shard_map/all_gather | solution.py:77
  127.3 172.2 %all-gather.15.cloned.1.call-start = ((), (), s32[]{:S(2)}) async-start(), calls=%async_computation.7 | async-start | bytes 10485760 | tf_op jit(solution)/shard_map/all_gather | solution.py:75
  127.9 321.0 %all-gather.17.cloned.1.call-start = ((), (), s32[]{:S(2)}) async-start(), calls=%async_computation.8 | async-start | bytes 10485760 | tf_op jit(solution)/shard_map/all_gather | solution.py:82
  128.6 367.9 %reduce-scatter.5.cloned.1.call-start = ((), (), s32[]{:S(2)}) async-start(), calls=%async_computation.9 | async-start | bytes 2621440 | tf_op jit(solution)/shard_map/reduce_scatter | solution.py:84
  465.4 31.1 %copy-start.2 = (bf16[128,2048]{1,0:T(8,128)(2,1)S(1)}, bf16[128,2048]{1,0:T(8,128)(2,1)}, u32[]{:S(2)}) copy-start(bf16[128,2048]{1,0:T(8,128)(2,1)} %reduce-scatter.3.cloned.1.call-done) | copy-start | bytes 1572868
Sparse Core Ops, SparseCore 0:
  8.9 27.4 all-gather.8
  38.0 22.8 all-gather.6
  62.4 27.0 all-gather.10
  93.0 30.9 reduce-scatter.2
  127.4 23.1 all-gather.12
  152.0 147.4 all-gather.14
  301.1 147.7 all-gather.16
  465.6 30.9 reduce-scatter.4
where the time goes:
time: 509 us; the launch traced here: 505 us
  waiting for transfers between devices  459 us (90%)
  matrix products  23 us (5%)
  between operations  13.6 us (3%)
  other arithmetic  9 us (2%)
    all_gather x1, waiting for transfers between devices, local(): down_local = lax.all_gather(down_weight, 'fs', axis=1, tiled=True)  149 us
    all_gather x1, waiting for transfers between devices, local(): up_local = lax.all_gather(up_weight, 'fs', axis=0, tiled=True)  149 us
    reduce_scatter x1, waiting for transfers between devices, local(): lax.psum_scatter(jnp.dot(block_rows, down_local, preferred_element_type=j...  31.1 us
    reduce_scatter x1, waiting for transfers between devices, local(): lax.psum_scatter(jnp.dot(block_rows, out_local, preferred_element_type=jn...  31 us
    all_gather x1, waiting for transfers between devices, local(): out_local = lax.all_gather(out_weight, 'fs', axis=1, tiled=True)  25.1 us
    all_gather x1, waiting for transfers between devices, local(): in_local = lax.all_gather(in_weight, 'fs', axis=0, tiled=True)  24.7 us
    all_gather x1, waiting for transfers between devices, local(): lax.all_gather(normed, 'tp', axis=0, tiled=True)  24.5 us
    all_gather x1, waiting for transfers between devices, local(): lax.all_gather(normed_two, 'tp', axis=0, tiled=True)  21.9 us
  transfers between devices with their start and end apart: 8, of which 8 were waited for; matrix products, arithmetic and copies ran while one was open for 1% of the time, Pallas kernels for 0%

commit v1 on v0

v1 whole, which is shorter than its diff:
```python
import functools

import jax
import jax.numpy as jnp
from jax import lax
from jax.experimental import pallas as pl
from jax.experimental.pallas import tpu as pltpu
from jax.sharding import PartitionSpec as P

MESH = pl.DeviceIdType.MESH
CHUNK_BYTES = 256 * 1024
LEVELS = 4

epsilon = 1e-06


def chunks_of(rows, columns, parts):
    count = max(1, rows * columns * 2 // parts // CHUNK_BYTES)
    while (rows // parts) % (count * 16):
        count -= 1
    return count


def dot(a, b):
    return jnp.dot(a, b, preferred_element_type=jnp.float32)


def tile_of(columns, most):
    tile = min(columns, most)
    while columns % tile:
        tile //= 2
    return tile


def kernel(
    sizes,
    tokens,
    gain1,
    in_hbm,
    group_weight,
    pool_scale,
    out_hbm,
    gain2,
    up_hbm,
    down_hbm,
    result,
    in_buf,
    out_buf,
    up_buf,
    down_buf,
    normed,
    projected,
    pool_out,
    mix_send,
    mix_recv,
    stream2,
    normed2,
    upper,
    hidden,
    sum_send,
    sum_recv,
    local_sem,
    in_sems,
    out_sems,
    up_sems,
    down_sems,
    tp_send,
    tp_recv,
):
    n_rep, n_fs, n_tp = sizes
    r, f, t = lax.axis_index("rep"), lax.axis_index("fs"), lax.axis_index("tp")
    rows = tokens.shape[0]
    length = rows * n_tp
    width = tokens.shape[1]
    part = width // n_fs
    buffers = (in_buf, out_buf, up_buf, down_buf)
    sources = (in_hbm, out_hbm, up_hbm, down_hbm)
    sems = (
        in_sems,
        out_sems,
        up_sems,
        down_sems,
    )
    chunk_counts = [chunks_of(b.shape[1], b.shape[2], n_rep) for b in buffers]

    loads = []
    for index in range(4):
        load = pltpu.make_async_copy(sources[index], buffers[index].at[f], local_sem.at[index])
        load.start()
        loads.append(load)

    barrier = pltpu.get_barrier_semaphore()
    greeted = [{"fs": lax.rem(f + d, n_fs)} for d in (1, n_fs - 1)]
    greeted += [{"rep": lax.rem(r + d, n_rep)} for d in range(1, n_rep)]
    greeted += [{"tp": lax.rem(t + d, n_tp)} for d in range(1, n_tp)]
    for device in greeted:
        pl.semaphore_signal(barrier, inc=1, device_id=device, device_id_type=MESH)

    def order(p):
        nearest = jnp.minimum(f, n_fs - 1 - f)
        step = (p + 1) // 2
        near = f + step if p % 2 else f - step
        far = f + (p - nearest) * jnp.where(2 * f < n_fs, 1, -1)
        return jnp.where(p <= 2 * nearest, near, far)

    def piece(g, j, q, c):
        buf = buffers[g]
        size = buf.shape[1] // n_rep // chunk_counts[g]
        start = pl.multiple_of((q * chunk_counts[g] + c) * size, size)
        return buf.at[j, pl.ds(start, size), :]

    def remote(g, j, q, c, send_slot, device):
        block = piece(g, j, q, c)
        return pltpu.make_async_remote_copy(
            src_ref=block,
            dst_ref=block,
            send_sem=sems[g].at[j, send_slot, c],
            recv_sem=sems[g].at[j, q, c],
            device_id=device,
            device_id_type=MESH,
        )

    def along(g, j, c, way, act):
        if way == 0:

            @pl.when(f > 0)
            def _():
                act(remote(g, j, r, c, 2 * n_rep, {"fs": f - 1}))

        else:

            @pl.when(f < n_fs - 1)
            def _():
                act(remote(g, j, r, c, 2 * n_rep + 1, {"fs": f + 1}))

    def start(copy):
        copy.start()

    def drain(copy):
        copy.wait_send()

    def onward(g, p, c, act):
        j = order(p)

        @pl.when(j > f)
        def _():
            along(g, j, c, 0, act)

        @pl.when(j < f)
        def _():
            along(g, j, c, 1, act)

        for d in range(1, n_rep):
            other = lax.rem(r + d, n_rep)
            act(remote(g, j, r, c, n_rep + other, {"rep": other}))

    def send_own(g):
        for c in range(chunk_counts[g]):
            along(g, f, c, 0, start)
            along(g, f, c, 1, start)

    def relay(g, p):
        for c in range(chunk_counts[g]):
            j = order(p)
            remote(g, j, r, c, 2 * n_rep, {"fs": f}).wait_recv()
            onward(g, p, c, start)

    def arrived(g, p):
        j = order(p)
        for d in range(1, n_rep):
            other = lax.rem(r + d, n_rep)
            for c in range(chunk_counts[g]):
                remote(g, j, other, c, n_rep + other, {"rep": other}).wait_recv()

    def block_of(index):
        return pl.ds(pl.multiple_of(index * rows, rows), rows)

    def tp_copies(kind, source, target):
        made = []
        for d in range(1, n_tp):
            other = lax.rem(t + d, n_tp)
            made.append(
                pltpu.make_async_remote_copy(
                    src_ref=source(other),
                    dst_ref=target(t),
                    send_sem=tp_send.at[kind, other],
                    recv_sem=tp_recv.at[kind, t],
                    device_id={"tp": other},
                    device_id_type=MESH,
                )
            )
        return made

    def tp_wait(kind, target):
        for d in range(1, n_tp):
            other = lax.rem(t + d, n_tp)
            pltpu.make_async_remote_copy(
                src_ref=target(other),
                dst_ref=target(other),
                send_sem=tp_send.at[kind, other],
                recv_sem=tp_recv.at[kind, other],
                device_id={"tp": other},
                device_id_type=MESH,
            ).wait_recv()

    stream = tokens[...].astype(jnp.float32)
    scale = lax.rsqrt(jnp.mean(stream * stream, axis=-1, keepdims=True) + epsilon)
    normed[block_of(t), :] = (stream * scale * gain1[...]).astype(jnp.bfloat16)

    pl.semaphore_wait(barrier, len(greeted))
    loads[0].wait()
    send_own(0)
    loads[1].wait()
    send_own(1)
    normed_at = lambda index: normed.at[block_of(index), :]
    sends = tp_copies(0, lambda other: normed_at(t), normed_at)
    for copy in sends:
        copy.start()
    for p in range(1, n_fs):
        relay(0, p)
        relay(1, p)
    loads[2].wait()
    send_own(2)

    tp_wait(0, normed_at)
    for p in range(1, n_fs):
        arrived(0, p)
    total = dot(normed[:, :part], in_buf[0])
    for index in range(1, n_fs):
        total += dot(normed[:, index * part : (index + 1) * part], in_buf[index])
    projected[...] = total.astype(jnp.bfloat16).astype(jnp.float32)
    groups, channels = group_weight.shape[0], group_weight.shape[1]
    position = lax.broadcasted_iota(jnp.int32, (length, channels), 0)
    for group in range(groups):
        lanes = slice(group * channels, (group + 1) * channels)
        values = projected[:, lanes]
        level_of = jnp.full((length, channels), lax.rem(t * groups + group, LEVELS), jnp.int32)
        running = values
        mean = jnp.zeros_like(values)
        for level in range(LEVELS):
            offset = 2**level
            running = running + jnp.where(position >= offset, pltpu.roll(running, offset, 0), 0.0)
            count = jnp.minimum(position + 1, 2 * offset).astype(jnp.float32)
            mean = jnp.where(level_of == level, running / count, mean)
        pooled = (mean - values).astype(jnp.bfloat16)
        mapped = dot(pooled, group_weight[group])
        pool_out[:, lanes] = (mapped * pool_scale[:, lanes]).astype(jnp.bfloat16)

    for p in range(1, n_fs):
        arrived(1, p)
    for index in range(n_fs):
        mix_send[index] = dot(pool_out[...], out_buf[index]).astype(jnp.bfloat16)
    more = tp_copies(
        1, lambda other: mix_send.at[:, block_of(other), :], lambda index: mix_recv.at[index]
    )
    relay(2, 1)
    for copy in more:
        copy.start()
    sends += more
    for p in range(2, n_fs - 1):
        relay(2, p)

    tp_wait(1, lambda index: mix_recv.at[index])
    square = jnp.zeros((rows, 1), jnp.float32)
    for index in range(n_fs):
        mixed = tokens[:, index * part : (index + 1) * part].astype(jnp.float32)
        mixed += mix_send[index, block_of(t), :].astype(jnp.float32)
        for d in range(1, n_tp):
            mixed += mix_recv[lax.rem(t + d, n_tp), index].astype(jnp.float32)
        stream2[index] = mixed
        square += jnp.sum(mixed * mixed, axis=-1, keepdims=True)
    scale = lax.rsqrt(square / width + epsilon)
    for index in range(n_fs):
        columns = slice(index * part, (index + 1) * part)
        normed2[block_of(t), columns] = (stream2[index] * scale * gain2[:, columns]).astype(
            jnp.bfloat16
        )
    normed2_at = lambda index: normed2.at[block_of(index), :]
    more = tp_copies(2, lambda other: normed2_at(t), normed2_at)
    for copy in more:
        copy.start()
    sends += more
    if n_fs > 2:
        relay(2, n_fs - 1)
    loads[3].wait()
    send_own(3)

    tp_wait(2, normed2_at)
    up_columns = up_buf.shape[2]
    up_tile = tile_of(up_columns, 512)

    def up_product(p):
        j = order(p)
        left = normed2.at[:, pl.ds(pl.multiple_of(j * part, part), part)]

        @pl.loop(0, up_columns // up_tile)
        def _(i):
            columns = pl.ds(pl.multiple_of(i * up_tile, up_tile), up_tile)
            product = dot(left[...], up_buf[j, :, columns])
            if p == 0:
                upper[:, columns] = product
            elif p < n_fs - 1:
                upper[:, columns] += product
            else:
                value = jnp.maximum(upper[:, columns] + product, 0.0)
                hidden[:, columns] = (value * value).astype(jnp.bfloat16)

    up_product(0)
    for p in range(1, n_fs):
        if p == n_fs - 1:
            relay(3, 1)
        arrived(2, p)
        up_product(p)

    down_tile = tile_of(part, 256)

    def sum_kind(p):
        return 3 + p

    def down_product(p):
        j = order(p)

        @pl.loop(0, part // down_tile)
        def _(i):
            columns = pl.ds(pl.multiple_of(i * down_tile, down_tile), down_tile)
            sum_send[p, :, columns] = dot(hidden[...], down_buf[j, :, columns]).astype(jnp.bfloat16)

        copies = tp_copies(
            sum_kind(p),
            lambda other: sum_send.at[p, block_of(other), :],
            lambda index: sum_recv.at[p, index],
        )
        for copy in copies:
            copy.start()
        return copies

    def finish(p):
        j = order(p)
        tp_wait(sum_kind(p), lambda index: sum_recv.at[p, index])
        channel = sum_send[p, block_of(t), :].astype(jnp.float32)
        for d in range(1, n_tp):
            channel += sum_recv[p, lax.rem(t + d, n_tp)].astype(jnp.float32)
        columns = pl.ds(pl.multiple_of(j * part, part), part)
        result[:, columns] = (stream2[j] + channel).astype(jnp.bfloat16)

    sends += down_product(0)
    for p in range(1, n_fs):
        if p < n_fs - 1:
            relay(3, p + 1)
        arrived(3, p)
        sends += down_product(p)
        finish(p - 1)
    for g in range(4):
        for c in range(chunk_counts[g]):
            along(g, f, c, 0, drain)
            along(g, f, c, 1, drain)
            for p in range(1, n_fs):
                onward(g, p, c, drain)
    finish(n_fs - 1)
    for copy in sends:
        copy.wait_send()


def local(sizes, tokens, gain1, in_w, group_w, pool_scale, out_w, gain2, up_w, down_w):
    n_rep, n_fs, n_tp = sizes
    rows, width = tokens.shape
    length, part = rows * n_tp, width // n_fs
    channels, hidden_units = in_w.shape[1], up_w.shape[1]
    bf16, f32 = jnp.bfloat16, jnp.float32
    weights = (in_w, out_w, up_w, down_w)
    vmem = pl.BlockSpec(memory_space=pltpu.VMEM)
    hbm = pl.BlockSpec(memory_space=pl.ANY)
    return pl.pallas_call(
        functools.partial(kernel, sizes),
        name="layer",
        out_shape=jax.ShapeDtypeStruct((rows, width), bf16),
        in_specs=[vmem, vmem, hbm, vmem, vmem, hbm, vmem, hbm, hbm],
        out_specs=vmem,
        scratch_shapes=[pltpu.VMEM((n_fs,) + w.shape, bf16) for w in weights]
        + [
            pltpu.VMEM((length, width), bf16),
            pltpu.VMEM((length, channels), f32),
            pltpu.VMEM((length, channels), bf16),
            pltpu.VMEM((n_fs, length, part), bf16),
            pltpu.VMEM((n_tp, n_fs, rows, part), bf16),
            pltpu.VMEM((n_fs, rows, part), f32),
            pltpu.VMEM((length, width), bf16),
            pltpu.VMEM((length, hidden_units), f32),
            pltpu.VMEM((length, hidden_units), bf16),
            pltpu.VMEM((n_fs, length, part), bf16),
            pltpu.VMEM((n_fs, n_tp, rows, part), bf16),
            pltpu.SemaphoreType.DMA((len(weights),)),
        ]
        + [
            pltpu.SemaphoreType.DMA((n_fs, 2 * n_rep + 2, chunks_of(*w.shape, n_rep)))
            for w in weights
        ]
        + [pltpu.SemaphoreType.DMA((3 + n_fs, n_tp))] * 2,
        compiler_params=pltpu.CompilerParams(
            collective_id=0, has_side_effects=True, vmem_limit_bytes=60 * 1024 * 1024
        ),
    )(
        tokens,
        gain1.reshape(1, -1),
        in_w,
        group_w,
        pool_scale.reshape(1, -1),
        out_w,
        gain2.reshape(1, -1),
        up_w,
        down_w,
    )


def solution(mesh):
    sizes = tuple(mesh.shape[axis] for axis in ("rep", "fs", "tp"))
    in_specs = (
        P(("rep", "fs", "tp"), None),
        P(),
        P("fs", "tp"),
        P("tp", None, None),
        P("tp"),
        P("tp", "fs"),
        P(),
        P("fs", "tp"),
        P("tp", "fs"),
    )
    return jax.shard_map(
        functools.partial(local, sizes),
        mesh=mesh,
        in_specs=in_specs,
        out_specs=P(("rep", "fs", "tp"), None),
        check_vma=False,
    )
```

time: 509 us -> 186 us (0.37)
  waiting for transfers between devices: 459 us -> 0 us
  Pallas kernels: 0 us -> 184 us
  matrix products: 23 us -> 0 us
  between operations: 13.6 us -> 0.01 us
  other arithmetic: 9 us -> 0 us
    all_gather x6 -> x0, waiting for transfers between devices: 394 us -> none  [the longest x1 149 us: local(): down_local = lax.all_gather(down_weight, 'fs', axis=1, tiled=True)]
    pallas_call x0 -> x1, Pallas kernels: none -> 184 us  [local(): pl.pallas_call(functools.partial(kernel, sizes), name='layer', out_shape=...]
    reduce_scatter x2 -> x0, waiting for transfers between devices: 62.1 us -> none  [the longest x1 31.1 us: local(): lax.psum_scatter(jnp.dot(block_rows, down_local, preferred_element_type=j...]
    dot_general x4 -> x0, matrix products: 23 us -> none  [the longest x1 16.5 us: local(): jnp.dot(block_rows, down_local, preferred_element_type=jnp.float32)]
    convert_element_type x6 -> x0, other arithmetic: 6.26 us -> none  [the longest x1 2.08 us: local(): return (mixed_stream + channel_sum).astype(jnp.bfloat16)]
  transfers between devices with their start and end apart: 8 -> 0, of which waited for: 8 -> 0; matrix products, arithmetic and copies ran while one was open for 1% -> 0% of each run, Pallas kernels for 0% -> 0%
where the time goes in v1:
time: 186 us
  Pallas kernels  184 us (99%)
  local copies, waits for them, and re-layouts  1.88 us (1%)
    pallas_call x1, Pallas kernels, local(): pl.pallas_call(functools.partial(kernel, sizes), name='layer', out_shape=...  184 us

profile of v1, /device:TPU:29, one launch (start us, length us, event | category | flops | bytes accessed | tf_op | source)
XLA Modules:
  0.0 185.6 jit_solution(13111315178949452569)
XLA Ops:
  0.0 183.8 %layer.1 = bf16[128,2048]{1,0:T(8,128)(2,1)} custom-call(bf16[128,2048]{1,0:T(8,128)(2,1)} %tokens.1, f32[1,2048]{1,0:T(1,128)} %bitcast.3, bf16[512,256]{1,0:T(8,128)(2,1)} %in_hbm.1, bf16[2,128,128]{2,1,0:T(8,128)(2,1)} %group_weight.1, f32[1,256]{1,0:T(1,128)} %bitcast.5, bf16[256,512]{1,0:T(8,128)(2,1)} %out_hbm.1, f32[1,2048]{1,0:T(1,128)} %bitcast.4, ...), custom_call_target="tpu_custom_call" | custom-call | tf_op jit(solution)/shard_map/layer/pallas_call | solution.py:373
  183.8 1.9 %copy.11 = bf16[128,2048]{1,0:T(8,128)(2,1)} copy(bf16[128,2048]{1,0:T(8,128)(2,1)} %layer.1) | data formatting | bytes 1048576

commit v2 on v1

--- a/solution.py
+++ b/solution.py
@@ -19,6 +19,18 @@
     while (rows // parts) % (count * 16):
         count -= 1
     return count
+
+
+def column_chunks(rows, columns, parts):
+    count = max(1, rows * columns * 2 // parts // CHUNK_BYTES)
+    while count > 1 and columns % (count * 128):
+        count -= 1
+    return count
+
+
+def chunk_counts_of(shapes, parts):
+    counts = [chunks_of(*shape, parts) for shape in shapes[:3]]
+    return counts + [column_chunks(*shapes[3], parts)]
 
 
 def dot(a, b):
@@ -81,7 +93,7 @@
         up_sems,
         down_sems,
     )
-    chunk_counts = [chunks_of(b.shape[1], b.shape[2], n_rep) for b in buffers]
+    chunk_counts = chunk_counts_of([b.shape[1:] for b in buffers], n_rep)
 
     loads = []
     for index in range(4):
@@ -105,6 +117,10 @@
 
     def piece(g, j, q, c):
         buf = buffers[g]
+        if g == 3:
+            half, block = buf.shape[1] // n_rep, buf.shape[2] // chunk_counts[g]
+            start = pl.multiple_of(q * half, half)
+            return buf.at[j, pl.ds(start, half), c * block : (c + 1) * block]
         size = buf.shape[1] // n_rep // chunk_counts[g]
         start = pl.multiple_of((q * chunk_counts[g] + c) * size, size)
         return buf.at[j, pl.ds(start, size), :]
@@ -133,6 +149,21 @@
             def _():
                 act(remote(g, j, r, c, 2 * n_rep + 1, {"fs": f + 1}))
 
+    def beside_end(j):
+        return ((j == 0) & (f == 1)) | ((j == n_fs - 1) & (f == n_fs - 2))
+
+    def whole_shard(g, c, act):
+        for d in range(1, n_rep):
+            other = lax.rem(r + d, n_rep)
+
+            @pl.when(f == 0)
+            def _():
+                act(remote(g, f, other, c, n_rep + other, {"fs": f + 1}))
+
+            @pl.when(f == n_fs - 1)
+            def _():
+                act(remote(g, f, other, c, n_rep + other, {"fs": f - 1}))
+
     def start(copy):
         copy.start()
 
@@ -150,20 +181,28 @@
         def _():
             along(g, j, c, 1, act)
 
-        for d in range(1, n_rep):
-            other = lax.rem(r + d, n_rep)
-            act(remote(g, j, r, c, n_rep + other, {"rep": other}))
+        @pl.when(jnp.logical_not(beside_end(j)))
+        def _():
+            for d in range(1, n_rep):
+                other = lax.rem(r + d, n_rep)
+                act(remote(g, j, r, c, n_rep + other, {"rep": other}))
 
     def send_own(g):
         for c in range(chunk_counts[g]):
             along(g, f, c, 0, start)
             along(g, f, c, 1, start)
-
-    def relay(g, p):
+        for c in range(chunk_counts[g]):
+            whole_shard(g, c, start)
+
+    def relay(g, p, work=()):
+        work = list(work)
         for c in range(chunk_counts[g]):
             j = order(p)
             remote(g, j, r, c, 2 * n_rep, {"fs": f}).wait_recv()
             onward(g, p, c, start)
+            if c < len(work):
+                for action in work[c]:
+                    action()
 
     def arrived(g, p):
         j = order(p)
@@ -253,12 +292,13 @@
     more = tp_copies(
         1, lambda other: mix_send.at[:, block_of(other), :], lambda index: mix_recv.at[index]
     )
-    relay(2, 1)
     for copy in more:
         copy.start()
     sends += more
-    for p in range(2, n_fs - 1):
+    for p in range(1, n_fs):
         relay(2, p)
+    loads[3].wait()
+    send_own(3)
 
     tp_wait(1, lambda index: mix_recv.at[index])
     square = jnp.zeros((rows, 1), jnp.float32)
@@ -280,10 +320,7 @@
     for copy in more:
         copy.start()
     sends += more
-    if n_fs > 2:
-        relay(2, n_fs - 1)
-    loads[3].wait()
-    send_own(3)
+    relay(3, 1)
 
     tp_wait(2, normed2_at)
     up_columns = up_buf.shape[2]
@@ -305,11 +342,9 @@
                 value = jnp.maximum(upper[:, columns] + product, 0.0)
                 hidden[:, columns] = (value * value).astype(jnp.bfloat16)
 
-    up_product(0)
-    for p in range(1, n_fs):
-        if p == n_fs - 1:
-            relay(3, 1)
-        arrived(2, p)
+    def up_work(p):
+        if p:
+            arrived(2, p)
         up_product(p)
 
     down_tile = tile_of(part, 256)
@@ -343,20 +378,78 @@
         columns = pl.ds(pl.multiple_of(j * part, part), part)
         result[:, columns] = (stream2[j] + channel).astype(jnp.bfloat16)
 
-    sends += down_product(0)
-    for p in range(1, n_fs):
-        if p < n_fs - 1:
-            relay(3, p + 1)
-        arrived(3, p)
-        sends += down_product(p)
-        finish(p - 1)
+    def down_work(p):
+        if p:
+            arrived(3, p)
+        sends.extend(down_product(p))
+        if p:
+            finish(p - 1)
+
+    count = chunk_counts[3]
+    block = part // count
+    last = n_fs - 1
+
+    def last_work(c):
+        j = order(last)
+        for d in range(1, n_rep):
+            other = lax.rem(r + d, n_rep)
+            remote(3, j, other, c, n_rep + other, {"rep": other}).wait_recv()
+        columns = slice(c * block, (c + 1) * block)
+        product = dot(hidden[...], down_buf[j, :, columns])
+        sum_send[last, :, columns] = product.astype(jnp.bfloat16)
+        copies = tp_copies(
+            sum_kind(last) + c,
+            lambda other: sum_send.at[last, block_of(other), columns],
+            lambda index: sum_recv.at[last, index, :, columns],
+        )
+        for copy in copies:
+            copy.start()
+        sends.extend(copies)
+
+    def last_finish(c):
+        j = order(last)
+        columns = slice(c * block, (c + 1) * block)
+        tp_wait(sum_kind(last) + c, lambda index: sum_recv.at[last, index, :, columns])
+        channel = sum_send[last, block_of(t), columns].astype(jnp.float32)
+        for d in range(1, n_tp):
+            channel += sum_recv[last, lax.rem(t + d, n_tp), :, columns].astype(jnp.float32)
+        place = pl.ds(pl.multiple_of(j * part + c * block, block), block)
+        result[:, place] = (stream2[j, :, columns] + channel).astype(jnp.bfloat16)
+
+    ups = [functools.partial(up_work, p) for p in range(n_fs)]
+    downs = [functools.partial(down_work, p) for p in range(last)]
+    lasts = [functools.partial(last_work, c) for c in range(count)]
+    for p in range(2, n_fs):
+        if ups:
+            step = -(-len(ups) // count)
+            relay(3, p, [ups[i : i + step] for i in range(0, len(ups), step)])
+            ups = []
+        elif p < last:
+            relay(3, p, [downs[:1]])
+            downs = downs[1:]
+        else:
+            plan = [[] for _ in range(count)]
+            half = (len(downs) + 1) // 2
+            plan[0] = downs[:half]
+            plan[min(1, count - 1)] = plan[min(1, count - 1)] + downs[half:]
+            if count == 1:
+                plan[0] = downs
+            for c in range(2, count):
+                plan[c] = [lasts.pop(0)]
+            relay(3, p, plan)
+            downs = []
+    for work in ups + downs + lasts:
+        work()
+    finish(last - 1)
     for g in range(4):
         for c in range(chunk_counts[g]):
             along(g, f, c, 0, drain)
             along(g, f, c, 1, drain)
+            whole_shard(g, c, drain)
             for p in range(1, n_fs):
                 onward(g, p, c, drain)
-    finish(n_fs - 1)
+    for c in range(count):
+        last_finish(c)
     for copy in sends:
         copy.wait_send()
 
@@ -368,6 +461,7 @@
     channels, hidden_units = in_w.shape[1], up_w.shape[1]
     bf16, f32 = jnp.bfloat16, jnp.float32
     weights = (in_w, out_w, up_w, down_w)
+    counts = chunk_counts_of([w.shape for w in weights], n_rep)
     vmem = pl.BlockSpec(memory_space=pltpu.VMEM)
     hbm = pl.BlockSpec(memory_space=pl.ANY)
     return pl.pallas_call(
@@ -392,10 +486,9 @@
             pltpu.SemaphoreType.DMA((len(weights),)),
         ]
         + [
-            pltpu.SemaphoreType.DMA((n_fs, 2 * n_rep + 2, chunks_of(*w.shape, n_rep)))
-            for w in weights
+            pltpu.SemaphoreType.DMA((n_fs, 2 * n_rep + 2, count)) for count in counts
         ]
-        + [pltpu.SemaphoreType.DMA((3 + n_fs, n_tp))] * 2,
+        + [pltpu.SemaphoreType.DMA((2 + n_fs + counts[3], n_tp))] * 2,
         compiler_params=pltpu.CompilerParams(
             collective_id=0, has_side_effects=True, vmem_limit_bytes=60 * 1024 * 1024
         ),

time: 186 us -> 186 us (level)
  Pallas kernels: 184 us -> 182 us
where the time goes in v2:
time: 186 us; the launch traced here: 184 us
  Pallas kernels  182 us (98%)
  local copies, waits for them, and re-layouts  1.88 us (1%)
    pallas_call x1, Pallas kernels, local(): pl.pallas_call(functools.partial(kernel, sizes), name='layer', out_shape=...  182 us

profile of v2, /device:TPU:29, one launch (start us, length us, event | category | flops | bytes accessed | tf_op | source)
XLA Modules:
  0.0 183.9 jit_solution(17125071147214966886)
XLA Ops:
  0.0 182.0 %layer.1 = bf16[128,2048]{1,0:T(8,128)(2,1)} custom-call(bf16[128,2048]{1,0:T(8,128)(2,1)} %tokens.1, f32[1,2048]{1,0:T(1,128)} %bitcast.3, bf16[512,256]{1,0:T(8,128)(2,1)} %in_hbm.1, bf16[2,128,128]{2,1,0:T(8,128)(2,1)} %group_weight.1, f32[1,256]{1,0:T(1,128)} %bitcast.5, bf16[256,512]{1,0:T(8,128)(2,1)} %out_hbm.1, f32[1,2048]{1,0:T(1,128)} %bitcast.4, ...), custom_call_target="tpu_custom_call" | custom-call | tf_op jit(solution)/shard_map/layer/pallas_call | solution.py:467
  182.0 1.9 %copy.11 = bf16[128,2048]{1,0:T(8,128)(2,1)} copy(bf16[128,2048]{1,0:T(8,128)(2,1)} %layer.1) | data formatting | bytes 1048576
